TPU v7x, 32 devices: a whole 2x2x4 slice. The times are simulated.
32 devices in a mesh: rep: 2 (over y), fs: 4 (over z), tp: 4 (over x, core).
Axes of the slice: x: 2, y: 2, z: 4, core: 2. Of those that a mesh axis runs over, the one named last changes fastest.
Arguments:
- activations: bfloat16 [2048, 4096], P(None, ('rep', 'fs')), may hold values from -60 to 60
- w_mix_in: bfloat16 [2048, 1024], P('fs', 'tp'), may hold values from -0.125 to 0.125
- w_mix_out: bfloat16 [2048, 1024], P('fs', 'tp'), may hold values from -0.1875 to 0.1875
- w_gate: bfloat16 [2048, 2816], P('fs', 'tp'), may hold values from -0.125 to 0.125
- w_up: bfloat16 [2048, 2816], P('fs', 'tp'), may hold values from -0.125 to 0.125
- w_down: bfloat16 [2048, 2816], P('fs', 'tp'), may hold values from -0.109375 to 0.109375
- pool_scale: float32 [1024], replicated, may hold values from 0.1 to 1.9
- gain_mix: float32 [2048], replicated, may hold values from 0.1 to 1.9
- gain_ffn: float32 [2048], replicated, may hold values from 0.1 to 1.9
- gain_out: float32 [2048], replicated, may hold values from 0.1 to 1.9
Outputs:
- normalized: bfloat16 [2048, 4096], P('tp', ('rep', 'fs'))
All inputs are finite; a program needn't handle non-finite values.
Results may differ from a plain program's by a relative error of at most 0.014.
Values may be sent and summed in bfloat16 or wider, within the bound.
A program may use at most 64 MiB of HBM per device.

v0:
```python
import jax
import jax.numpy as jnp
from jax import lax
from jax.sharding import PartitionSpec as P

POOL_GROUP = 256
SEQ_LEN = 256


EPS = 1e-06
WINDOWS = (2, 4, 8, 16)


def rms_factor(stream):
    return lax.rsqrt(jnp.mean(stream * stream, axis=0, keepdims=True) + EPS)


def pool_tokens(inputs, group_of):
    channels = inputs.shape[0]
    values = inputs.astype(jnp.float32).reshape(channels, -1, SEQ_LEN)
    sequences = values.shape[1]
    running = jnp.concatenate(
        [jnp.zeros((channels, sequences, 1), jnp.float32), jnp.cumsum(values, axis=-1)], axis=-1
    )
    places = jnp.arange(SEQ_LEN, dtype=jnp.int32)
    pooled_sum = jnp.zeros_like(values)
    for group_id, window in enumerate(WINDOWS):
        behind = window // 2
        onward = window - behind
        upper_sum = jnp.concatenate(
            [running, jnp.repeat(running[..., -1:], onward, axis=-1)], axis=-1
        )[..., onward : onward + SEQ_LEN]
        lower_sum = jnp.concatenate(
            [jnp.zeros((channels, sequences, behind), jnp.float32), running], axis=-1
        )[..., :SEQ_LEN]
        counts = (jnp.minimum(places + onward, SEQ_LEN) - jnp.maximum(places - behind, 0)).astype(
            jnp.float32
        )
        window_mean = (upper_sum - lower_sum) / counts
        pooled_sum = pooled_sum + jnp.where((group_of == group_id)[:, None, None], window_mean, 0.0)
    return (pooled_sum - values).reshape(channels, -1)


def contract_first(weights, acts):
    return lax.dot_general(
        weights, acts, (((0,), (0,)), ((), ())), preferred_element_type=jnp.float32
    )


def on_device(
    activations, w_mix_in, w_mix_out, w_gate, w_up, w_down, pool_scale, gain_mix, gain_ffn, gain_out
):
    group_size = lax.axis_size("tp")
    group_rank = lax.axis_index("tp")
    features = activations.shape[0]
    feature_share = features // group_size
    feature_start = group_rank * feature_share
    stream = activations.astype(jnp.float32)
    normed = (stream * rms_factor(stream) * gain_mix[:, None]).astype(jnp.bfloat16)
    in_full, out_full = (
        lax.all_gather(w_mix_in, "fs", axis=0, tiled=True),
        lax.all_gather(w_mix_out, "fs", axis=0, tiled=True),
    )
    inputs = contract_first(in_full, normed).astype(jnp.bfloat16)
    channel_share = w_mix_in.shape[1]
    channel_ids = group_rank * channel_share + jnp.arange(channel_share, dtype=jnp.int32)
    group_of = channel_ids // POOL_GROUP
    scale_own = lax.dynamic_slice_in_dim(pool_scale, group_rank * channel_share, channel_share)
    pooled = (pool_tokens(inputs, group_of) * scale_own[:, None]).astype(jnp.bfloat16)
    mixed = lax.psum(
        jnp.dot(out_full, pooled, preferred_element_type=jnp.float32).astype(jnp.bfloat16), "tp"
    ).astype(jnp.float32)
    after_mix = lax.optimization_barrier((stream + mixed).astype(jnp.bfloat16)).astype(jnp.float32)
    normed_two = (after_mix * rms_factor(after_mix) * gain_ffn[:, None]).astype(jnp.bfloat16)
    after_own = lax.dynamic_slice_in_dim(after_mix, feature_start, feature_share, 0)
    gate_full, up_full, down_full = (
        lax.all_gather(w_gate, "fs", axis=0, tiled=True),
        lax.all_gather(w_up, "fs", axis=0, tiled=True),
        lax.all_gather(w_down, "fs", axis=0, tiled=True),
    )
    gate = contract_first(gate_full, normed_two)
    upward = contract_first(up_full, normed_two)
    hidden = (jax.nn.silu(gate) * upward).astype(jnp.bfloat16)
    ffn_own = lax.psum_scatter(
        jnp.dot(down_full, hidden, preferred_element_type=jnp.float32).astype(jnp.bfloat16),
        "tp",
        scatter_dimension=0,
        tiled=True,
    ).astype(jnp.float32)
    final_own = after_own + ffn_own
    final_squares = lax.psum(jnp.sum(final_own * final_own, axis=0), "tp")
    final_factor = lax.rsqrt(final_squares / features + EPS)
    gain_last = lax.dynamic_slice_in_dim(gain_out, feature_start, feature_share)
    return (final_own * final_factor[None, :] * gain_last[:, None]).astype(jnp.bfloat16)


def solution(mesh):
    placed = (
        P(None, ("rep", "fs")),
        P("fs", "tp"),
        P("fs", "tp"),
        P("fs", "tp"),
        P("fs", "tp"),
        P("fs", "tp"),
        P(),
        P(),
        P(),
        P(),
    )
    return jax.shard_map(
        on_device, mesh=mesh, in_specs=placed, out_specs=P("tp", ("rep", "fs")), check_vma=False
    )
```

profile of v0, /device:TPU:0, one launch (start us, length us, event | category | flops | bytes accessed | tf_op | source)
XLA Modules:
  0.0 356.4 jit_solution(6297903444097482954)
XLA Ops:
  6.5 0.0 all-gather.6.cloned.1.call-start
  6.5 0.7 all-gather.6.cloned.1.call-update
  7.3 0.0 all-gather.8.cloned.1.call-start
  7.3 0.7 all-gather.8.cloned.1.call-update
  8.0 0.0 all-reduce.2.cloned.1.call-start
  8.1 0.0 copy-start.1
  8.1 2.9 copy.14
  11.1 0.0 copy-start
  11.1 0.5 fusion
  11.6 0.8 dynamic_slice.9
  12.4 27.2 %all-gather.6.cloned.1.call-done = bf16[2048,256]{1,0:T(8,128)(2,1)} async-done(((bf16[512,256]{1,0:T(8,128)(2,1)}), bf16[2048,256]{1,0:T(8,128)(2,1)}) %all-gather.6.cloned.1.call-update) | async-done | bytes 1048592 | tf_op jit(solution)/shard_map/all_gather | solution.py:61
  39.6 0.0 copy-done.1
  39.6 2.0 fusion.15
  41.6 0.0 copy-done
  41.6 0.4 fusion.35
  42.1 0.2 broadcast_add_fusion
  42.3 0.1 copy.16
  42.5 0.8 fusion.22
  43.3 25.3 %all-gather.8.cloned.1.call-done = bf16[2048,256]{1,0:T(8,128)(2,1)} async-done(((bf16[512,256]{1,0:T(8,128)(2,1)}), bf16[2048,256]{1,0:T(8,128)(2,1)}) %all-gather.8.cloned.1.call-update) | async-done | bytes 1048592 | tf_op jit(solution)/shard_map/all_gather | solution.py:62
  68.6 3.3 fusion.4
  71.9 0.0 all-reduce.2.cloned.1.call-update
  71.9 0.0 all-gather.10.cloned.1.call-start
  72.0 0.5 all-gather.10.cloned.1.call-update
  72.5 0.0 all-gather.14.cloned.1.call-start
  72.6 0.5 all-gather.14.cloned.1.call-update
  73.1 0.0 all-gather.12.cloned.1.call-start
  73.1 0.5 all-gather.12.cloned.1.call-update
  73.7 0.0 copy-start.2
  73.7 0.0 reduce-scatter.2.cloned.1.call-start
  73.7 49.1 %all-reduce.2.cloned.1.call-done = bf16[2048,512]{0,1:T(8,128)(2,1)} async-done(((bf16[2048,512]{0,1:T(8,128)(2,1)}), bf16[2048,512]{0,1:T(8,128)(2,1)}) %all-reduce.2.cloned.1.call-update) | async-done | bytes 2097168 | tf_op jit(solution)/shard_map/psum | solution.py:70
  122.8 3.0 fusion.3
  125.8 0.5 multiply_reduce_fusion
  126.3 57.1 %all-gather.10.cloned.1.call-done = bf16[2048,704]{0,1:T(8,128)(2,1)} async-done(((bf16[512,704]{0,1:T(8,128)(2,1)}), bf16[2048,704]{0,1:T(8,128)(2,1)}) %all-gather.10.cloned.1.call-update) | async-done | bytes 2883600 | tf_op jit(solution)/shard_map/all_gather | solution.py:77
  183.5 0.0 copy-done.2
  183.5 3.6 %convolution_bitcast_fusion.1 = f32[704,512]{1,0:T(8,128)S(1)} fusion(bf16[2048,704]{0,1:T(8,128)(2,1)} %all-gather.10.cloned.1.call-done, f32[2048]{0:T(1024)S(1)} %copy-done.2, f32[512]{0:T(512)S(1)} %add_rsqrt_fusion.1, bf16[2048,512]{0,1:T(8,128)(2,1)S(1)} %fusion.3), kind=kOutput, calls=%fused_computation.18 | convolution fusion | flops 1480589312 | bytes 6432768 | tf_op jit(solution)/shard_map/dot_general | solution.py:45
  187.1 55.7 %all-gather.14.cloned.1.call-done = bf16[2048,704]{0,1:T(8,128)(2,1)} async-done(((bf16[512,704]{0,1:T(8,128)(2,1)}), bf16[2048,704]{0,1:T(8,128)(2,1)}) %all-gather.14.cloned.1.call-update) | async-done | bytes 2883600 | tf_op jit(solution)/shard_map/all_gather | solution.py:79
  242.7 59.3 %all-gather.12.cloned.1.call-done = bf16[2048,704]{0,1:T(8,128)(2,1)} async-done(((bf16[512,704]{0,1:T(8,128)(2,1)}), bf16[2048,704]{0,1:T(8,128)(2,1)}) %all-gather.12.cloned.1.call-update) | async-done | bytes 2883600 | tf_op jit(solution)/shard_map/all_gather | solution.py:78
  302.0 7.6 %fusion.5 = bf16[2048,512]{0,1:T(8,128)(2,1)} fusion(bf16[2048,704]{0,1:T(8,128)(2,1)} %all-gather.14.cloned.1.call-done, bf16[2048,704]{0,1:T(8,128)(2,1)} %all-gather.12.cloned.1.call-done, f32[704,512]{1,0:T(8,128)S(1)} %convolution_bitcast_fusion.1, f32[2048]{0:T(1024)S(1)} %copy-done.2, f32[512]{0:T(512)S(1)} %add_rsqrt_fusion.1, ...), kind=kOutput, calls=%fused_computation.12 | convolution fusion | flops 2960195584 | bytes 11413504 | tf_op jit(solution)/shard_map/dot_general | solution.py:85
  309.6 0.0 reduce-scatter.2.cloned.1.call-update
  309.6 0.8 dynamic_slice.11
  310.4 2.5 convert_element_type.94
  312.9 26.8 %reduce-scatter.2.cloned.1.call-done = bf16[512,512]{0,1:T(8,128)(2,1)} async-done(((bf16[2048,512]{0,1:T(8,128)(2,1)}), bf16[512,512]{0,1:T(8,128)(2,1)}) %reduce-scatter.2.cloned.1.call-update) | async-done | bytes 524304 | tf_op jit(solution)/shard_map/reduce_scatter | solution.py:84
  339.6 1.6 multiply_reduce_fusion.1
  341.2 5.8 %psum.15 = f32[512]{0:T(512)S(1)} all-reduce(f32[512]{0:T(512)S(1)} %multiply_reduce_fusion.1), channel_id=1, replica_groups=mesh['rep'=2,'fs'=4,'tp'=4] {'tp'}, use_global_device_ids=true, to_apply=%region_7.8 | all-reduce | flops 512 | bytes 4096 | tf_op jit(solution)/shard_map/psum | solution.py:91
  347.0 1.6 multiply_convert_fusion.1
  348.6 1.0 copy.17
  (22 shorter events, 0.2 us)
Async XLA Ops:
  6.5 33.1 %all-gather.6.cloned.1.call-start = ((), (), s32[]{:S(2)}) async-start(), calls=%async_computation.1 | async-start | bytes 1310720 | tf_op jit(solution)/shard_map/all_gather | solution.py:61
  7.3 61.3 %all-gather.8.cloned.1.call-start = ((), (), s32[]{:S(2)}) async-start(), calls=%async_computation.2 | async-start | bytes 1310720 | tf_op jit(solution)/shard_map/all_gather | solution.py:62
  8.0 114.8 %all-reduce.2.cloned.1.call-start = ((), (), s32[]{:S(2)}) async-start(), calls=%async_computation.3 | async-start | bytes 4194304 | tf_op jit(solution)/shard_map/psum | solution.py:70
  8.1 31.5 %copy-start.1 = (f32[2048]{0:T(1024)S(1)}, f32[2048]{0:T(1024)}, u32[]{:S(2)}) copy-start(f32[2048]{0:T(1024)} %param.17) | copy-start | bytes 24580
  11.1 30.6 %copy-start = (bf16[2048,512]{0,1:T(8,128)(2,1)}, bf16[2048,512]{0,1:T(8,128)(2,1)S(1)}, u32[]{:S(2)}) copy-start(bf16[2048,512]{0,1:T(8,128)(2,1)S(1)} %copy.14) | copy-start | bytes 6291460
  71.9 111.6 %all-gather.10.cloned.1.call-start = ((), (), s32[]{:S(2)}) async-start(), calls=%async_computation.4 | async-start | bytes 3604480 | tf_op jit(solution)/shard_map/all_gather | solution.py:77
  72.5 170.2 %all-gather.14.cloned.1.call-start = ((), (), s32[]{:S(2)}) async-start(), calls=%async_computation.6 | async-start | bytes 3604480 | tf_op jit(solution)/shard_map/all_gather | solution.py:79
  73.1 228.9 %all-gather.12.cloned.1.call-start = ((), (), s32[]{:S(2)}) async-start(), calls=%async_computation.5 | async-start | bytes 3604480 | tf_op jit(solution)/shard_map/all_gather | solution.py:78
  73.7 109.8 %copy-start.2 = (f32[2048]{0:T(1024)S(1)}, f32[2048]{0:T(1024)}, u32[]{:S(2)}) copy-start(f32[2048]{0:T(1024)} %param.18) | copy-start | bytes 24580
  73.7 266.0 %reduce-scatter.2.cloned.1.call-start = ((), (), s32[]{:S(2)}) async-start(), calls=%async_computation.7 | async-start | bytes 2621440 | tf_op jit(solution)/shard_map/reduce_scatter | solution.py:84
Sparse Core Ops, SparseCore 0:
  8.9 30.6 all-gather.5
  41.2 27.3 all-gather.7
  72.1 50.7 all-reduce.1
  124.3 59.1 all-gather.9
  184.9 57.7 all-gather.13
  244.2 57.7 all-gather.11
  309.7 29.8 reduce-scatter.1
where the time goes:
time: 357 us; the launch traced here: 356 us
  waiting for transfers between devices  303 us (85%)
  matrix products  16.5 us (5%)
  between operations  13.7 us (4%)
  other arithmetic  11.1 us (3%)
  blocking collectives  5.76 us (2%)
  local copies, waits for them, and re-layouts  5.68 us (2%)
    all_gather x1, waiting for transfers between devices, on_device(): lax.all_gather(w_up, 'fs', axis=0, tiled=True)  59.3 us
    all_gather x1, waiting for transfers between devices, on_device(): lax.all_gather(w_gate, 'fs', axis=0, tiled=True)  57.1 us
    all_gather x1, waiting for transfers between devices, on_device(): lax.all_gather(w_down, 'fs', axis=0, tiled=True)  55.7 us
    psum x1, waiting for transfers between devices, on_device(): lax.psum(jnp.dot(out_full, pooled, preferred_element_type=jnp.float32).as...  49.1 us
    all_gather x1, waiting for transfers between devices, on_device(): lax.all_gather(w_mix_in, 'fs', axis=0, tiled=True)  27.2 us
    reduce_scatter x1, waiting for transfers between devices, on_device(): lax.psum_scatter(jnp.dot(down_full, hidden, preferred_element_type=jnp.fl...  26.8 us
    all_gather x1, waiting for transfers between devices, on_device(): lax.all_gather(w_mix_out, 'fs', axis=0, tiled=True)  25.3 us
    dot_general x1, matrix products, on_device(): jnp.dot(down_full, hidden, preferred_element_type=jnp.float32)  7.61 us
  transfers between devices with their start and end apart: 7, of which 7 were waited for; matrix products, arithmetic and copies ran while one was open for 5% of the time, Pallas kernels for 0%

commit v1 on v0

v1 whole, which is shorter than its diff:
```python
import functools

import jax
import jax.numpy as jnp
from jax import lax
from jax.experimental import pallas as pl
from jax.experimental.pallas import tpu as pltpu
from jax.sharding import PartitionSpec as P

POOL_GROUP = 256
SEQ_LEN = 256
EPS = 1e-06
LANES = 128
MESH = pl.DeviceIdType.MESH
BF = jnp.bfloat16
F32 = jnp.float32


def dot_first(weights, acts):
    return lax.dot_general(weights, acts, (((0,), (0,)), ((), ())), preferred_element_type=F32)


def column(row, width):
    square = jnp.transpose(jnp.broadcast_to(row, (LANES, LANES)))
    return jnp.concatenate([square] * (width // LANES), axis=1)


def body(
    nr, nf, nt,
    act, w_in, w_out, w_gate, w_up, w_down, scale, g_mix, g_ffn, g_out, out,
    b_in, b_out, b_gate, b_up, b_down,
    h, x1, part0, part1, u_acc, pooled, gate_acc, up_acc, hidden, own_x, squares,
    buf_a, buf_b,
    own_sem, zsend, zrecv, ysend, yrecv,
    a_send, a_recv, b_send, b_recv, c_send, c_recv, d_send, d_recv, s_send, s_recv,
):
    r, f, t = lax.axis_index("rep"), lax.axis_index("fs"), lax.axis_index("tp")
    features, tokens = act.shape
    shards = (w_in, w_out, w_gate, w_up, w_down)
    full = (b_in, b_out, b_gate, b_up, b_down)
    rows = w_in.shape[0]
    piece = rows // nr
    share = features // nt
    channels = w_in.shape[1]
    ff = w_gate.shape[1]
    nh = nt // 2
    chip, parity = t // 2, lax.rem(t, 2)
    partner = t + 1 - 2 * parity

    own = [pltpu.make_async_copy(shards[m], full[m].at[f], own_sem.at[m]) for m in range(5)]
    for copy in own:
        copy.start()

    barrier = pltpu.get_barrier_semaphore()
    for step in (1, nf - 1):
        pl.semaphore_signal(barrier, inc=1, device_id=(r, lax.rem(f + step, nf), t), device_id_type=MESH)
    for o in range(1, nr):
        pl.semaphore_signal(barrier, inc=1, device_id=(lax.rem(r + o, nr), f, t), device_id_type=MESH)
    for i in range(1, nt):
        pl.semaphore_signal(barrier, inc=1, device_id=(r, f, lax.rem(t + i, nt)), device_id_type=MESH)
    pl.semaphore_wait(barrier, 2 + (nr - 1) + (nt - 1))

    def z_copy(m, blk, way, d):
        ref = full[m].at[blk, pl.ds(pl.multiple_of(r * piece, piece), piece), :]
        return pltpu.make_async_remote_copy(
            src_ref=ref, dst_ref=ref,
            send_sem=zsend.at[m, way, lax.rem(d, 2)], recv_sem=zrecv.at[m, blk],
            device_id=(r, f + 1 - 2 * way, t), device_id_type=MESH,
        )

    def y_copy(m, blk, way, d, o):
        ref = full[m].at[blk, pl.ds(pl.multiple_of(r * piece, piece), piece), :]
        return pltpu.make_async_remote_copy(
            src_ref=ref, dst_ref=ref,
            send_sem=ysend.at[m, way, lax.rem(d, 2), o - 1], recv_sem=yrecv.at[m, blk, o - 1],
            device_id=(lax.rem(r + o, nr), f, t), device_id_type=MESH,
        )

    def y_arrival(m, blk, o):
        source = lax.rem(r - o + nr, nr)
        ref = full[m].at[blk, pl.ds(pl.multiple_of(source * piece, piece), piece), :]
        return pltpu.make_async_remote_copy(
            src_ref=ref, dst_ref=ref,
            send_sem=ysend.at[m, 0, 0, o - 1], recv_sem=yrecv.at[m, blk, o - 1],
            device_id=(lax.rem(r + o, nr), f, t), device_id_type=MESH,
        )

    can_send = (f + 1 < nf, f >= 1)
    hops = (f, nf - 1 - f)

    def send_own(m):
        own[m].wait()
        for way in (0, 1):
            @pl.when(can_send[way])
            def _():
                z_copy(m, f, way, 0).start()

    def arrival(m, way, d):
        blk = f - d if way == 0 else f + d

        @pl.when(d <= hops[way])
        def _():
            z_copy(m, blk, way, d).wait_recv()

            @pl.when(can_send[way])
            def _():
                @pl.when(d >= 2)
                def _():
                    z_copy(m, blk, way, d).wait_send()

                z_copy(m, blk, way, d).start()

            for o in range(1, nr):
                @pl.when(d >= 3)
                def _():
                    y_copy(m, blk, way, d, o).wait_send()

                y_copy(m, blk, way, d, o).start()

    def gather(m, low, high):
        if low >= high:
            return

        def rounds(d, carry):
            arrival(m, 0, d)
            arrival(m, 1, d)
            return carry

        if low == 1:
            rounds(jnp.int32(1), 0)
            if m + 2 < 5:
                send_own(m + 2)
            low = 2
        lax.fori_loop(low, high, rounds, 0)

    def finish(m):
        def one(blk, carry):
            @pl.when(blk != f)
            def _():
                for o in range(1, nr):
                    y_arrival(m, blk, o).wait_recv()
            return carry

        lax.fori_loop(0, nf, one, 0)

    def drain(m):
        for way in (0, 1):
            for back in (0, 1):
                last = hops[way] - back

                @pl.when(jnp.logical_and(can_send[way], last >= 0))
                def _():
                    z_copy(m, f, way, last).wait_send()

                @pl.when(last >= 1)
                def _():
                    for o in range(1, nr):
                        y_copy(m, f, way, last, o).wait_send()

    def share_of(ref, j):
        return ref.at[pl.ds(pl.multiple_of(j * share, share), share), :]

    def normalize(load, gain, store, count):
        def square(i, total):
            v = load(i)
            return total + jnp.sum(v * v, axis=0, keepdims=True)

        total = lax.fori_loop(0, count, square, jnp.zeros((1, tokens), F32))
        factor = lax.rsqrt(total / features + EPS)

        def scaled(i, carry):
            store(i, load(i) * factor * column(gain[pl.ds(i, 1), :], tokens))
            return carry

        lax.fori_loop(0, count, scaled, 0)

    def chunk(ref, i):
        return ref[pl.ds(pl.multiple_of(i * LANES, LANES), LANES), :].astype(F32)

    def put(ref):
        def store(i, v):
            ref[pl.ds(pl.multiple_of(i * LANES, LANES), LANES), :] = v.astype(ref.dtype)
        return store

    def a_copy(k, part, c):
        return pltpu.make_async_remote_copy(
            src_ref=share_of(part, 2 * c + 1 - parity), dst_ref=buf_a.at[k, c],
            send_sem=a_send.at[k, c], recv_sem=a_recv.at[k, c],
            device_id=(r, f, partner), device_id_type=MESH,
        )

    def b_copy(k, part, i):
        target = 2 * lax.rem(chip + i, nh) + parity
        return pltpu.make_async_remote_copy(
            src_ref=share_of(part, target), dst_ref=buf_b.at[k, i],
            send_sem=b_send.at[k, i], recv_sem=b_recv.at[k, i],
            device_id=(r, f, target), device_id_type=MESH,
        )

    def start_pair(k, part):
        for i in range(nh):
            a_copy(k, part, i).start()

    def start_chips(k, part):
        for c in range(nh):
            a_copy(k, part, c).wait()
        for i in range(1, nh):
            c = lax.rem(chip + i, nh)
            target = 2 * c + parity

            def add(n, carry):
                at = pl.ds(pl.multiple_of(target * share + n * LANES, LANES), LANES)
                mine = part[at, :].astype(F32)
                theirs = buf_a[k, c, pl.ds(pl.multiple_of(n * LANES, LANES), LANES), :].astype(F32)
                part[at, :] = (mine + theirs).astype(BF)
                return carry

            lax.fori_loop(0, share // LANES, add, 0)
            b_copy(k, part, i).start()

    def finish_chips(k, part, base, store):
        for i in range(1, nh):
            b_copy(k, part, i).wait()

        def add(n, carry):
            here = pl.ds(pl.multiple_of(n * LANES, LANES), LANES)
            at = pl.ds(pl.multiple_of(t * share + n * LANES, LANES), LANES)
            total = part[at, :].astype(F32) + buf_a[k, chip, here, :].astype(F32)
            for i in range(1, nh):
                total = total + buf_b[k, i, here, :].astype(F32)
            store(n, base[at, :].astype(F32) + total)
            return carry

        lax.fori_loop(0, share // LANES, add, 0)

    def c_copy(i):
        ref = share_of(x1, t)
        return pltpu.make_async_remote_copy(
            src_ref=ref, dst_ref=ref, send_sem=c_send.at[i], recv_sem=c_recv.at[i],
            device_id=(r, f, 2 * lax.rem(chip + i, nh) + parity), device_id_type=MESH,
        )

    def d_copy(i):
        ref = share_of(x1, 2 * lax.rem(chip - i + nh, nh) + parity)
        return pltpu.make_async_remote_copy(
            src_ref=ref, dst_ref=ref, send_sem=d_send.at[i], recv_sem=d_recv.at[i],
            device_id=(r, f, partner), device_id_type=MESH,
        )

    def s_copy(i):
        return pltpu.make_async_remote_copy(
            src_ref=squares.at[0], dst_ref=squares.at[i], send_sem=s_send.at[i], recv_sem=s_recv.at[i],
            device_id=(r, f, lax.rem(t + i, nt)), device_id_type=MESH,
        )

    send_own(0)
    send_own(1)
    normalize(functools.partial(chunk, act), g_mix, put(h), features // LANES)

    gather(0, 1, nf)
    finish(0)
    u_acc[...] = jnp.zeros_like(u_acc)

    def mix_in(b, carry):
        at = pl.ds(pl.multiple_of(b * rows, rows), rows)
        u_acc[...] += dot_first(b_in[b], h[at, :])
        return carry

    lax.fori_loop(0, nf, mix_in, 0)
    for i in range(channels // LANES):
        first = t * channels + i * LANES
        window = jnp.int32(2) << (first // POOL_GROUP)
        behind = window // 2
        onward = window - behind
        source = lax.broadcasted_iota(jnp.int32, (SEQ_LEN, SEQ_LEN), 0)
        place = lax.broadcasted_iota(jnp.int32, (SEQ_LEN, SEQ_LEN), 1)
        inside = jnp.logical_and(source >= place - behind, source < place + onward)
        band = jnp.where(inside, 1.0, 0.0).astype(BF)
        spot = lax.broadcasted_iota(jnp.int32, (1, SEQ_LEN), 1)
        count = (jnp.minimum(spot + onward, SEQ_LEN) - jnp.maximum(spot - behind, 0)).astype(F32)
        gain = column(scale[pl.ds(first // LANES, 1), :], SEQ_LEN)
        for s in range(tokens // SEQ_LEN):
            at = (pl.ds(i * LANES, LANES), pl.ds(s * SEQ_LEN, SEQ_LEN))
            u = u_acc[at].astype(BF)
            mean = jnp.dot(u, band, preferred_element_type=F32) / count
            pooled[at] = ((mean - u.astype(F32)) * gain).astype(BF)

    gather(1, 1, nf)
    finish(1)

    def mix_out(b, carry):
        at = pl.ds(pl.multiple_of(b * rows, rows), rows)
        part0[at, :] = jnp.dot(b_out[b], pooled[...], preferred_element_type=F32).astype(BF)
        return carry

    lax.fori_loop(0, nf, mix_out, 0)
    start_pair(0, part0)
    third = 1 + (nf - 1) // 3
    gather(2, 1, third)
    start_chips(0, part0)
    gather(2, third, nf)

    def keep_x1(n, v):
        at = pl.ds(pl.multiple_of(t * share + n * LANES, LANES), LANES)
        x1[at, :] = v.astype(BF)

    finish_chips(0, part0, act, keep_x1)
    for i in range(1, nh):
        c_copy(i).start()
    d_copy(0).start()
    far = 1 + 2 * (nf - 1) // 3
    gather(3, 1, far)
    for i in range(1, nh):
        c_copy(i).wait()
        d_copy(i).start()
    gather(3, far, nf)
    for i in range(nh):
        d_copy(i).wait()
    normalize(functools.partial(chunk, x1), g_ffn, put(h), features // LANES)
    finish(2)
    gate_acc[...] = jnp.zeros_like(gate_acc)
    up_acc[...] = jnp.zeros_like(up_acc)

    def project(source, acc):
        def one(b, carry):
            at = pl.ds(pl.multiple_of(b * rows, rows), rows)
            acc[...] += dot_first(source[b], h[at, :])
            return carry

        lax.fori_loop(0, nf, one, 0)

    project(b_gate, gate_acc)
    gather(4, 1, third)
    finish(3)
    project(b_up, up_acc)
    gather(4, third, far)
    step = 32

    def activate(n, carry):
        at = pl.ds(pl.multiple_of(n * step, step), step)
        v = gate_acc[at, :]
        hidden[at, :] = (v / (1.0 + jnp.exp(-v)) * up_acc[at, :]).astype(BF)
        return carry

    lax.fori_loop(0, ff // step, activate, 0)
    gather(4, far, nf)
    finish(4)

    def mlp_out(b, carry):
        at = pl.ds(pl.multiple_of(b * rows, rows), rows)
        part1[at, :] = jnp.dot(b_down[b], hidden[...], preferred_element_type=F32).astype(BF)
        return carry

    lax.fori_loop(0, nf, mlp_out, 0)
    start_pair(1, part1)
    for m in range(5):
        drain(m)
    start_chips(1, part1)
    finish_chips(1, part1, x1, put(own_x))

    def square(i, total):
        v = chunk(own_x, i)
        return total + jnp.sum(v * v, axis=0, keepdims=True)

    mine = lax.fori_loop(0, share // LANES, square, jnp.zeros((1, tokens), F32))
    squares[0] = jnp.broadcast_to(mine, squares.shape[1:])
    for i in range(1, nt):
        s_copy(i).start()
    for i in range(1, nt):
        s_copy(i).wait()
    total = squares[0, pl.ds(0, 1), :]
    for i in range(1, nt):
        total = total + squares[i, pl.ds(0, 1), :]
    factor = lax.rsqrt(total / features + EPS)

    def closing(i, carry):
        gain = column(g_out[pl.ds(t * (share // LANES) + i, 1), :], tokens)
        put(out)(i, chunk(own_x, i) * factor * gain)
        return carry

    lax.fori_loop(0, share // LANES, closing, 0)


def solution(mesh):
    nr, nf, nt = mesh.shape["rep"], mesh.shape["fs"], mesh.shape["tp"]

    def on_device(act, w_in, w_out, w_gate, w_up, w_down, scale, g_mix, g_ffn, g_out):
        features, tokens = act.shape
        rows, channels = w_in.shape
        ff = w_gate.shape[1]
        share = features // nt
        nh = nt // 2
        anywhere = pl.BlockSpec(memory_space=pl.ANY)
        vmem = pl.BlockSpec(memory_space=pltpu.VMEM)
        dma = pltpu.SemaphoreType.DMA
        scratch = [
            pltpu.VMEM((nf, rows, channels), BF),
            pltpu.VMEM((nf, rows, channels), BF),
            pltpu.VMEM((nf, rows, ff), BF),
            pltpu.VMEM((nf, rows, ff), BF),
            pltpu.VMEM((nf, rows, ff), BF),
            pltpu.VMEM((features, tokens), BF),
            pltpu.VMEM((features, tokens), BF),
            pltpu.VMEM((features, tokens), BF),
            pltpu.VMEM((features, tokens), BF),
            pltpu.VMEM((channels, tokens), F32),
            pltpu.VMEM((channels, tokens), BF),
            pltpu.VMEM((ff, tokens), F32),
            pltpu.VMEM((ff, tokens), F32),
            pltpu.VMEM((ff, tokens), BF),
            pltpu.VMEM((share, tokens), F32),
            pltpu.VMEM((nt, 8, tokens), F32),
            pltpu.VMEM((2, nh, share, tokens), BF),
            pltpu.VMEM((2, nh, share, tokens), BF),
            dma((5,)),
            dma((5, 2, 2)),
            dma((5, nf)),
            dma((5, 2, 2, max(nr - 1, 1))),
            dma((5, nf, max(nr - 1, 1))),
            dma((2, nh)), dma((2, nh)), dma((2, nh)), dma((2, nh)),
            dma((nh,)), dma((nh,)), dma((nh,)), dma((nh,)),
            dma((nt,)), dma((nt,)),
        ]
        return pl.pallas_call(
            functools.partial(body, nr, nf, nt),
            out_shape=jax.ShapeDtypeStruct((share, tokens), BF),
            in_specs=[vmem] + [anywhere] * 5 + [vmem] * 4,
            out_specs=vmem,
            scratch_shapes=scratch,
            compiler_params=pltpu.CompilerParams(
                collective_id=0, has_side_effects=True, vmem_limit_bytes=60 * 1024 * 1024
            ),
        )(
            act, w_in, w_out, w_gate, w_up, w_down,
            *[v.reshape(-1, LANES) for v in (scale, g_mix, g_ffn, g_out)],
        )

    weight = P("fs", "tp")
    tokens_split = P(None, ("rep", "fs"))
    return jax.shard_map(
        on_device,
        mesh=mesh,
        in_specs=(tokens_split, *[weight] * 5, P(), P(), P(), P()),
        out_specs=P("tp", ("rep", "fs")),
        check_vma=False,
    )
```

time: 357 us -> 157 us (0.44)
  waiting for transfers between devices: 303 us -> 0 us
  Pallas kernels: 0 us -> 149 us
  matrix products: 16.5 us -> 0 us
  between operations: 13.7 us -> 0.01 us
  other arithmetic: 11.1 us -> 0 us
  blocking collectives: 5.76 us -> 0 us
    all_gather x5 -> x0, waiting for transfers between devices: 225 us -> none  [the longest x1 59.3 us: on_device(): lax.all_gather(w_up, 'fs', axis=0, tiled=True)]
    pallas_call x0 -> x1, Pallas kernels: none -> 149 us  [on_device(): pl.pallas_call(functools.partial(body, nr, nf, nt), out_shape=jax.ShapeDt...]
    psum x1 -> x0, waiting for transfers between devices: 49.1 us -> none  [on_device(): lax.psum(jnp.dot(out_full, pooled, preferred_element_type=jnp.float32).as...]
    reduce_scatter x1 -> x0, waiting for transfers between devices: 26.8 us -> none  [on_device(): lax.psum_scatter(jnp.dot(down_full, hidden, preferred_element_type=jnp.fl...]
    dot_general x4 -> x0, matrix products: 16.5 us -> none  [the longest x1 7.61 us: on_device(): jnp.dot(down_full, hidden, preferred_element_type=jnp.float32)]
    convert_element_type x6 -> x0, other arithmetic: 7.09 us -> none  [the longest x1 3.01 us: on_device(): (stream + mixed).astype(jnp.bfloat16)]
    psum x1 -> x0, blocking collectives: 5.76 us -> none  [on_device(): final_squares = lax.psum(jnp.sum(final_own * final_own, axis=0), 'tp')]
    unnamed x8 -> x6, local copies, waits for them, and re-layouts: 2.95 us -> 7.67 us
  transfers between devices with their start and end apart: 7 -> 0, of which waited for: 7 -> 0; matrix products, arithmetic and copies ran while one was open for 5% -> 0% of each run, Pallas kernels for 0% -> 0%
where the time goes in v1:
time: 157 us
  Pallas kernels  149 us (95%)
  local copies, waits for them, and re-layouts  7.67 us (5%)
    pallas_call x1, Pallas kernels, on_device(): pl.pallas_call(functools.partial(body, nr, nf, nt), out_shape=jax.ShapeDt...  149 us
    unnamed x6, local copies, waits for them, and re-layouts  7.67 us

profile of v1, /device:TPU:0, one launch (start us, length us, event | category | flops | bytes accessed | tf_op | source)
XLA Modules:
  0.0 157.0 jit_solution(11466852505780340106)
XLA Ops:
  0.0 0.0 copy-start
  0.0 2.3 %copy.11.w_gate = bf16[512,704]{1,0:T(8,128)(2,1)} copy(bf16[512,704]{0,1:T(8,128)(2,1)} %param.13) | data formatting | bytes 1441792 | tf_op args[3]
  2.3 2.3 %copy.12.w_up = bf16[512,704]{1,0:T(8,128)(2,1)} copy(bf16[512,704]{0,1:T(8,128)(2,1)} %param.14) | data formatting | bytes 1441792 | tf_op args[4]
  4.6 0.0 copy-done
  4.6 1.2 copy.13.w_down
  5.8 149.3 %shard_map.100 = bf16[512,512]{1,0:T(8,128)(2,1)} custom-call(bf16[2048,512]{1,0:T(8,128)(2,1)} %act.1, bf16[512,256]{1,0:T(8,128)(2,1)} %w_in.1, bf16[512,256]{1,0:T(8,128)(2,1)} %w_out.1, bf16[512,704]{1,0:T(8,128)(2,1)} %copy.11.w_gate, bf16[512,704]{1,0:T(8,128)(2,1)} %copy.12.w_up, bf16[512,704]{1,0:T(8,128)(2,1)} %copy.13.w_down, f32[8,128]{1,0:T(8,128)} %bitcast.7, ...), custom_call_target="tpu_custom_call" | custom-call | tf_op jit(solution)/shard_map/pallas_call | solution.py:424
  155.2 1.9 %copy.15 = bf16[512,512]{1,0:T(8,128)(2,1)} copy(bf16[512,512]{1,0:T(8,128)(2,1)} %shard_map.100) | data formatting | bytes 1048576
Async XLA Ops:
  0.0 4.6 %copy-start = (bf16[512,704]{0,1:T(8,128)(2,1)S(1)}, bf16[512,704]{0,1:T(8,128)(2,1)}, u32[]{:S(2)}) copy-start(bf16[512,704]{0,1:T(8,128)(2,1)} %param.15) | copy-start | bytes 2162692

commit v2 on v1

--- a/solution.py
+++ b/solution.py
@@ -47,6 +47,11 @@
     chip, parity = t // 2, lax.rem(t, 2)
     partner = t + 1 - 2 * parity
 
+    cut = -(-ff // (2 * LANES)) * LANES
+    items = [(0, 0, channels), (1, 0, channels)]
+    for m in (2, 3, 4):
+        items += [(m, 0, cut), (m, cut, ff - cut)]
+
     own = [pltpu.make_async_copy(shards[m], full[m].at[f], own_sem.at[m]) for m in range(5)]
     for copy in own:
         copy.start()
@@ -60,8 +65,13 @@
         pl.semaphore_signal(barrier, inc=1, device_id=(r, f, lax.rem(t + i, nt)), device_id_type=MESH)
     pl.semaphore_wait(barrier, 2 + (nr - 1) + (nt - 1))
 
+    def part_of(m, blk, of):
+        matrix, start, size = items[m]
+        at = pl.ds(pl.multiple_of(of * piece, piece), piece)
+        return full[matrix].at[blk, at, pl.ds(start, size)]
+
     def z_copy(m, blk, way, d):
-        ref = full[m].at[blk, pl.ds(pl.multiple_of(r * piece, piece), piece), :]
+        ref = part_of(m, blk, r)
         return pltpu.make_async_remote_copy(
             src_ref=ref, dst_ref=ref,
             send_sem=zsend.at[m, way, lax.rem(d, 2)], recv_sem=zrecv.at[m, blk],
@@ -69,7 +79,7 @@
         )
 
     def y_copy(m, blk, way, d, o):
-        ref = full[m].at[blk, pl.ds(pl.multiple_of(r * piece, piece), piece), :]
+        ref = part_of(m, blk, r)
         return pltpu.make_async_remote_copy(
             src_ref=ref, dst_ref=ref,
             send_sem=ysend.at[m, way, lax.rem(d, 2), o - 1], recv_sem=yrecv.at[m, blk, o - 1],
@@ -78,7 +88,7 @@
 
     def y_arrival(m, blk, o):
         source = lax.rem(r - o + nr, nr)
-        ref = full[m].at[blk, pl.ds(pl.multiple_of(source * piece, piece), piece), :]
+        ref = part_of(m, blk, source)
         return pltpu.make_async_remote_copy(
             src_ref=ref, dst_ref=ref,
             send_sem=ysend.at[m, 0, 0, o - 1], recv_sem=yrecv.at[m, blk, o - 1],
@@ -89,7 +99,8 @@
     hops = (f, nf - 1 - f)
 
     def send_own(m):
-        own[m].wait()
+        if items[m][1] == 0:
+            own[items[m][0]].wait()
         for way in (0, 1):
             @pl.when(can_send[way])
             def _():
@@ -128,8 +139,8 @@
 
         if low == 1:
             rounds(jnp.int32(1), 0)
-            if m + 2 < 5:
-                send_own(m + 2)
+            if m + 1 < len(items):
+                send_own(m + 1)
             low = 2
         lax.fori_loop(low, high, rounds, 0)
 
@@ -202,11 +213,10 @@
             a_copy(k, part, i).start()
 
     def start_chips(k, part):
-        for c in range(nh):
-            a_copy(k, part, c).wait()
         for i in range(1, nh):
             c = lax.rem(chip + i, nh)
             target = 2 * c + parity
+            a_copy(k, part, c).wait()
 
             def add(n, carry):
                 at = pl.ds(pl.multiple_of(target * share + n * LANES, LANES), LANES)
@@ -219,6 +229,7 @@
             b_copy(k, part, i).start()
 
     def finish_chips(k, part, base, store):
+        a_copy(k, part, chip).wait()
         for i in range(1, nh):
             b_copy(k, part, i).wait()
 
@@ -254,10 +265,10 @@
         )
 
     send_own(0)
-    send_own(1)
     normalize(functools.partial(chunk, act), g_mix, put(h), features // LANES)
 
     gather(0, 1, nf)
+    gather(1, 1, nf)
     finish(0)
     u_acc[...] = jnp.zeros_like(u_acc)
 
@@ -285,7 +296,7 @@
             mean = jnp.dot(u, band, preferred_element_type=F32) / count
             pooled[at] = ((mean - u.astype(F32)) * gain).astype(BF)
 
-    gather(1, 1, nf)
+    gather(2, 1, nf)
     finish(1)
 
     def mix_out(b, carry):
@@ -295,10 +306,9 @@
 
     lax.fori_loop(0, nf, mix_out, 0)
     start_pair(0, part0)
-    third = 1 + (nf - 1) // 3
-    gather(2, 1, third)
+    gather(3, 1, nf)
     start_chips(0, part0)
-    gather(2, third, nf)
+    gather(4, 1, nf)
 
     def keep_x1(n, v):
         at = pl.ds(pl.multiple_of(t * share + n * LANES, LANES), LANES)
@@ -308,16 +318,16 @@
     for i in range(1, nh):
         c_copy(i).start()
     d_copy(0).start()
-    far = 1 + 2 * (nf - 1) // 3
-    gather(3, 1, far)
+    gather(5, 1, nf)
     for i in range(1, nh):
         c_copy(i).wait()
         d_copy(i).start()
-    gather(3, far, nf)
+    gather(6, 1, nf)
     for i in range(nh):
         d_copy(i).wait()
     normalize(functools.partial(chunk, x1), g_ffn, put(h), features // LANES)
     finish(2)
+    finish(3)
     gate_acc[...] = jnp.zeros_like(gate_acc)
     up_acc[...] = jnp.zeros_like(up_acc)
 
@@ -329,11 +339,11 @@
 
         lax.fori_loop(0, nf, one, 0)
 
+    gather(7, 1, nf)
     project(b_gate, gate_acc)
-    gather(4, 1, third)
-    finish(3)
+    finish(4)
+    finish(5)
     project(b_up, up_acc)
-    gather(4, third, far)
     step = 32
 
     def activate(n, carry):
@@ -343,19 +353,33 @@
         return carry
 
     lax.fori_loop(0, ff // step, activate, 0)
-    gather(4, far, nf)
-    finish(4)
+    finish(6)
+    finish(7)
 
     def mlp_out(b, carry):
         at = pl.ds(pl.multiple_of(b * rows, rows), rows)
         part1[at, :] = jnp.dot(b_down[b], hidden[...], preferred_element_type=F32).astype(BF)
         return carry
 
-    lax.fori_loop(0, nf, mlp_out, 0)
-    start_pair(1, part1)
-    for m in range(5):
+    if share % rows == 0:
+        blocks = share // rows
+
+        def pair_out(c):
+            theirs, ours = 2 * c + 1 - parity, 2 * c + parity
+            lax.fori_loop(theirs * blocks, (theirs + 1) * blocks, mlp_out, 0)
+            a_copy(1, part1, c).start()
+            lax.fori_loop(ours * blocks, (ours + 1) * blocks, mlp_out, 0)
+
+        for i in range(1, nh):
+            pair_out(lax.rem(chip + i, nh))
+        start_chips(1, part1)
+        pair_out(chip)
+    else:
+        lax.fori_loop(0, nf, mlp_out, 0)
+        start_pair(1, part1)
+        start_chips(1, part1)
+    for m in range(len(items)):
         drain(m)
-    start_chips(1, part1)
     finish_chips(1, part1, x1, put(own_x))
 
     def square(i, total):
@@ -413,10 +437,10 @@
             pltpu.VMEM((2, nh, share, tokens), BF),
             pltpu.VMEM((2, nh, share, tokens), BF),
             dma((5,)),
-            dma((5, 2, 2)),
-            dma((5, nf)),
-            dma((5, 2, 2, max(nr - 1, 1))),
-            dma((5, nf, max(nr - 1, 1))),
+            dma((8, 2, 2)),
+            dma((8, nf)),
+            dma((8, 2, 2, max(nr - 1, 1))),
+            dma((8, nf, max(nr - 1, 1))),
             dma((2, nh)), dma((2, nh)), dma((2, nh)), dma((2, nh)),
             dma((nh,)), dma((nh,)), dma((nh,)), dma((nh,)),
             dma((nt,)), dma((nt,)),

time: 157 us -> 141 us (0.90)
  Pallas kernels: 149 us -> 133 us
    pallas_call x1, Pallas kernels: 149 us -> 133 us  [on_device(): pl.pallas_call(functools.partial(body, nr, nf, nt), out_shape=jax.ShapeDt...]
where the time goes in v2:
time: 141 us
  Pallas kernels  133 us (94%)
  local copies, waits for them, and re-layouts  7.67 us (5%)
    pallas_call x1, Pallas kernels, on_device(): pl.pallas_call(functools.partial(body, nr, nf, nt), out_shape=jax.ShapeDt...  133 us
    unnamed x6, local copies, waits for them, and re-layouts  7.67 us

profile of v2, /device:TPU:0, one launch (start us, length us, event | category | flops | bytes accessed | tf_op | source)
XLA Modules:
  0.0 140.6 jit_solution(14266252826345036438)
XLA Ops:
  0.0 0.0 copy-start
  0.0 2.3 %copy.11.w_gate = bf16[512,704]{1,0:T(8,128)(2,1)} copy(bf16[512,704]{0,1:T(8,128)(2,1)} %param.13) | data formatting | bytes 1441792 | tf_op args[3]
  2.3 2.3 %copy.12.w_up = bf16[512,704]{1,0:T(8,128)(2,1)} copy(bf16[512,704]{0,1:T(8,128)(2,1)} %param.14) | data formatting | bytes 1441792 | tf_op args[4]
  4.6 0.0 copy-done
  4.6 1.2 copy.13.w_down
  5.8 132.9 %shard_map.100 = bf16[512,512]{1,0:T(8,128)(2,1)} custom-call(bf16[2048,512]{1,0:T(8,128)(2,1)} %act.1, bf16[512,256]{1,0:T(8,128)(2,1)} %w_in.1, bf16[512,256]{1,0:T(8,128)(2,1)} %w_out.1, bf16[512,704]{1,0:T(8,128)(2,1)} %copy.11.w_gate, bf16[512,704]{1,0:T(8,128)(2,1)} %copy.12.w_up, bf16[512,704]{1,0:T(8,128)(2,1)} %copy.13.w_down, f32[8,128]{1,0:T(8,128)} %bitcast.7, ...), custom_call_target="tpu_custom_call" | custom-call | tf_op jit(solution)/shard_map/pallas_call | solution.py:448
  138.8 1.9 %copy.15 = bf16[512,512]{1,0:T(8,128)(2,1)} copy(bf16[512,512]{1,0:T(8,128)(2,1)} %shard_map.100) | data formatting | bytes 1048576
Async XLA Ops:
  0.0 4.6 %copy-start = (bf16[512,704]{0,1:T(8,128)(2,1)S(1)}, bf16[512,704]{0,1:T(8,128)(2,1)}, u32[]{:S(2)}) copy-start(bf16[512,704]{0,1:T(8,128)(2,1)} %param.15) | copy-start | bytes 2162692
